TPU v7x, 32 devices: a whole 2x2x4 slice. The times are simulated.
32 devices in a mesh: sp: 16 (over z, y, x), tp: 2 (over core).
Axes of the slice: x: 2, y: 2, z: 4, core: 2. Of those that a mesh axis runs over, the one named last changes fastest.
Arguments:
- resid: bfloat16 [3072, 2048], P('sp'), may hold values from -6 to 6
- query: bfloat16 [3072, 2048], P('sp', 'tp'), may hold values from -6 to 6
- key: bfloat16 [3072, 1024], P('sp', 'tp'), may hold values from -6 to 6
- value: bfloat16 [3072, 1024], P('sp', 'tp'), may hold values from -6 to 6
- q_gain: float32 [128], replicated, may hold values from 0.3 to 5, as said below
- k_gain: float32 [128], replicated, may hold values from 0.3 to 5, as said below
- out_weight: bfloat16 [2048, 2048], P('tp'), may hold values from -0.125 to 0.125
- norm_gain: float32 [2048], replicated, may hold values from 0.1 to 1.9
- gate_weight: bfloat16 [2048, 5632], P('sp', 'tp'), may hold values from -0.125 to 0.125
- up_weight: bfloat16 [2048, 5632], P('sp', 'tp'), may hold values from -0.125 to 0.125
- down_weight: bfloat16 [5632, 2048], P('tp', 'sp'), may hold values from -0.078125 to 0.078125
Outputs:
- mixed: bfloat16 [3072, 2048], P(('sp', 'tp'))
Inputs may be any that keep to these rules, and one draw needn't show every extreme that they name: `q_gain`: positive gains. `k_gain`: positive gains.
All inputs are finite; a program needn't handle non-finite values.
Results may differ from a plain program's by a relative error of at most 0.012.
The roundings to bfloat16 on the way count: a program that leaves them out, or rounds other values in their place, can miss the bound.
Values may be sent and summed in bfloat16 or wider, within the bound.
A program may use at most 128 MiB of HBM per device.

v0:
```python
import jax
import jax.numpy as jnp
from jax import lax
from jax.sharding import PartitionSpec as P

GRID_W = 64
EPSILON = 1e-06


def rotate(values, positions):
    dim_size = values.shape[-1]
    half_dim = dim_size // 2
    quarter = half_dim // 2
    inverse = 10000.0 ** (-jnp.arange(quarter, dtype=jnp.float32) / quarter)
    outputs = []
    for axis_pos, coords in enumerate((positions // GRID_W, positions % GRID_W)):
        angles = coords.astype(jnp.float32)[:, None] * inverse[None, :]
        cosine = jnp.cos(angles)[:, None, :]
        sine = jnp.sin(angles)[:, None, :]
        section = values[..., axis_pos * half_dim : (axis_pos + 1) * half_dim]
        first_half = section[..., :quarter]
        second_half = section[..., quarter:]
        outputs += [
            first_half * cosine - second_half * sine,
            second_half * cosine + first_half * sine,
        ]
    return jnp.concatenate(outputs, axis=-1)


def prepare(projected, gain, positions):
    values = projected.astype(jnp.float32)
    normed = values * lax.rsqrt(jnp.mean(values * values, axis=-1, keepdims=True) + EPSILON) * gain
    return rotate(normed, positions).astype(jnp.bfloat16)


def normalize(stream, gain):
    values = stream.astype(jnp.float32)
    return (
        values * lax.rsqrt(jnp.mean(values * values, axis=-1, keepdims=True) + EPSILON) * gain
    ).astype(jnp.bfloat16)


def body(
    resid,
    query,
    key,
    value,
    q_gain,
    k_gain,
    out_weight,
    norm_gain,
    gate_weight,
    up_weight,
    down_weight,
):
    rows_here = query.shape[0]
    head_dim = q_gain.shape[0]
    heads_here = query.shape[1] // head_dim
    kv_here = key.shape[1] // head_dim
    group_size = heads_here // kv_here
    score_scale = head_dim ** (-0.5)
    positions = lax.axis_index("sp") * rows_here + jnp.arange(rows_here, dtype=jnp.int32)
    q_rot = prepare(query.reshape(rows_here, heads_here, head_dim), q_gain, positions)
    k_rot = prepare(key.reshape(rows_here, kv_here, head_dim), k_gain, positions)
    val_rows = value.reshape(rows_here, kv_here, head_dim)
    grouped = q_rot.reshape(rows_here, kv_here, group_size, head_dim)

    def key_block(carry, block):
        maxima, totals, accum = carry
        block_keys, block_vals = block
        scores = (
            jnp.einsum("qkgd,skd->kgqs", grouped, block_keys, preferred_element_type=jnp.float32)
            * score_scale
        )
        new_max = jnp.maximum(maxima, jnp.max(scores, axis=-1))
        shrink = jnp.exp(maxima - new_max)
        weights = jnp.exp(scores - new_max[..., None])
        totals = totals * shrink + jnp.sum(weights, axis=-1)
        accum = accum * shrink[..., None] + jnp.einsum(
            "kgqs,skd->kgqd",
            weights.astype(jnp.bfloat16),
            block_vals,
            preferred_element_type=jnp.float32,
        )
        return ((new_max, totals, accum), None)

    start_max = jnp.full((kv_here, group_size, rows_here), -1e30, jnp.float32)
    start_total = jnp.zeros((kv_here, group_size, rows_here), jnp.float32)
    start_accum = jnp.zeros((kv_here, group_size, rows_here, head_dim), jnp.float32)
    carry = (start_max, start_total, start_accum)
    key_part = lax.all_gather(k_rot, "sp", axis=0, tiled=True)
    val_part = lax.all_gather(val_rows, "sp", axis=0, tiled=True)
    length = key_part.shape[0]
    factor = 4
    span = rows_here * factor
    turns = length // span
    key_blocks = key_part.reshape(turns, span, kv_here, head_dim)
    val_blocks = val_part.reshape(turns, span, kv_here, head_dim)
    carry, _ = lax.scan(key_block, carry, (key_blocks, val_blocks))
    maxima, totals, accum = carry
    attn = (
        jnp.transpose(accum / totals[..., None], (2, 0, 1, 3))
        .reshape(rows_here, heads_here * head_dim)
        .astype(jnp.bfloat16)
    )
    share = rows_here // lax.axis_size("tp")
    my_first = lax.axis_index("tp") * share
    proj = lax.psum_scatter(
        jnp.dot(attn, out_weight, preferred_element_type=jnp.float32).astype(jnp.bfloat16),
        "tp",
        scatter_dimension=0,
        tiled=True,
    ).astype(jnp.float32)
    my_resid = lax.dynamic_slice_in_dim(resid, my_first, share, 0)
    my_stream = (my_resid.astype(jnp.float32) + proj).astype(jnp.bfloat16)
    mixer_rows = lax.all_gather(normalize(my_stream, norm_gain), "tp", axis=0, tiled=True)

    def add_rows(shard_rows):
        return jnp.dot(mixer_rows, shard_rows, preferred_element_type=jnp.float32)

    gate = add_rows(lax.all_gather(gate_weight, "sp", axis=0, tiled=True))
    up_part = add_rows(lax.all_gather(up_weight, "sp", axis=0, tiled=True))
    hidden = (jax.nn.silu(gate) * up_part).astype(jnp.bfloat16)
    down_whole = lax.all_gather(down_weight, "sp", axis=1, tiled=True)
    down = lax.psum_scatter(
        jnp.dot(hidden, down_whole, preferred_element_type=jnp.float32).astype(jnp.bfloat16),
        "tp",
        scatter_dimension=0,
        tiled=True,
    ).astype(jnp.float32)
    return (my_stream.astype(jnp.float32) + 0.5 * down).astype(jnp.bfloat16)


def solution(mesh):
    placed = (
        P("sp", None),
        P("sp", "tp"),
        P("sp", "tp"),
        P("sp", "tp"),
        P(),
        P(),
        P("tp", None),
        P(),
        P("sp", "tp"),
        P("sp", "tp"),
        P("tp", "sp"),
    )
    return jax.shard_map(
        body, mesh=mesh, in_specs=placed, out_specs=P(("sp", "tp"), None), check_vma=False
    )
```

profile of v0, /device:TPU:0, one launch (start us, length us, event | category | flops | bytes accessed | tf_op | source)
XLA Modules:
  0.0 702.4 jit_solution(25329568361684075)
XLA Ops:
  6.6 1.1 reshape.193
  7.7 0.3 multiply_reduce_fusion.1
  8.0 0.9 multiply_multiply_fusion.1
  8.9 0.8 multiply_cosine_fusion.1
  9.7 0.7 subtract_convert_fusion.3
  10.4 1.3 pad_maximum_fusion.1
  11.8 0.7 reshape.191
  12.9 0.3 multiply_reduce_fusion
  13.4 0.3 multiply_multiply_fusion
  13.6 0.7 subtract_convert_fusion.1
  14.6 0.5 pad_maximum_fusion
  15.1 67.4 %all-gather.6.cloned.1.call-done = bf16[3072,4,128]{2,1,0:T(4,128)(2,1)} async-done(((bf16[192,4,128]{2,1,0:T(4,128)(2,1)}), bf16[3072,4,128]{2,1,0:T(4,128)(2,1)}) %all-gather.6.cloned.1.call-update) | async-done | bytes 3145744 | tf_op jit(solution)/shard_map/all_gather | solution.py:91
  82.5 69.2 %all-gather.8.cloned.1.call-done = bf16[3072,4,128]{2,1,0:T(4,128)(2,1)} async-done(((bf16[192,4,128]{2,1,0:T(4,128)(2,1)}), bf16[3072,4,128]{2,1,0:T(4,128)(2,1)}) %all-gather.8.cloned.1.call-update) | async-done | bytes 3145744 | tf_op jit(solution)/shard_map/all_gather | solution.py:92
  151.7 40.1 %while.15 = (s32[]{:T(128)}, f32[4,2,192]{2,1,0:T(2,128)S(1)}, f32[4,2,192]{2,1,0:T(2,128)S(1)}, f32[4,2,192,128]{3,2,1,0:T(8,128)S(1)}, bf16[4,768,4,128]{3,2,1...) while((s32[]{:T(128)}, f32[4,2,192]{2,1,0:T(2,128)S(1)}, ...), condition=%wide.region_5.6_spmd.clone, body=%wide.region_2.5_spmd.clone.sunk | while | flops 614014464 | bytes 39813256 | solution.py:99
  151.7 1.9 constant_dynamic-slice_fusion.3
  153.6 2.9 bitcast_reduce_fusion.2
  156.5 3.5 fusion.42
  160.1 0.2 copy-done
  160.3 1.4 fusion.44
  161.7 1.9 constant_dynamic-slice_fusion.3
  163.6 2.9 bitcast_reduce_fusion.2
  166.6 3.5 fusion.42
  170.3 1.4 fusion.44
  171.7 1.9 constant_dynamic-slice_fusion.3
  173.6 2.9 bitcast_reduce_fusion.2
  176.6 3.5 fusion.42
  180.3 1.4 fusion.44
  181.7 1.9 constant_dynamic-slice_fusion.3
  183.7 2.9 bitcast_reduce_fusion.2
  186.6 3.5 fusion.42
  190.3 1.4 fusion.44
  191.8 0.3 fusion.19
  192.0 0.4 copy.56
  192.5 0.3 convert_element_type.83
  192.8 4.1 convolution_convert_fusion.1
  196.9 0.5 all-gather.10.cloned.1.call-update
  197.5 0.5 all-gather.12.cloned.1.call-update
  198.1 0.5 all-gather.14.cloned.1.call-update
  198.7 5.1 reduce-scatter.3.cloned.1.call-done
  203.8 1.2 fusion.15
  205.2 2.5 all_gather.20
  207.7 141.2 %all-gather.10.cloned.1.call-done = bf16[2048,2816]{1,0:T(8,128)(2,1)} async-done(((bf16[128,2816]{1,0:T(8,128)(2,1)}), bf16[2048,2816]{1,0:T(8,128)(2,1)}) %all-gather.10.cloned.1.call-update) | async-done | bytes 11534352 | tf_op jit(solution)/shard_map/all_gather | solution.py:121
  348.9 6.7 fusion.24
  355.6 135.6 %all-gather.12.cloned.1.call-done = bf16[2048,2816]{1,0:T(8,128)(2,1)} async-done(((bf16[128,2816]{1,0:T(8,128)(2,1)}), bf16[2048,2816]{1,0:T(8,128)(2,1)}) %all-gather.12.cloned.1.call-update) | async-done | bytes 11534352 | tf_op jit(solution)/shard_map/all_gather | solution.py:122
  491.2 182.8 %all-gather.14.cloned.1.call-done = bf16[2816,2048]{1,0:T(8,128)(2,1)} async-done(((bf16[2816,128]{1,0:T(8,128)(2,1)}), bf16[2816,2048]{1,0:T(8,128)(2,1)}) %all-gather.14.cloned.1.call-update) | async-done | bytes 11534352 | tf_op jit(solution)/shard_map/all_gather | solution.py:124
  674.0 13.2 %convolution_convert_fusion = bf16[192,2048]{1,0:T(8,128)(2,1)} fusion(bf16[2816,2048]{1,0:T(8,128)(2,1)} %all-gather.14.cloned.1.call-done, bf16[192,2048]{1,0:T(8,128)(2,1)S(1)} %all_gather.20, bf16[2048,2816]{1,0:T(8,128)(2,1)} %all-gather.12.cloned.1.call-done, f32[192,2816]{1,0:T(8,128)S(1)} %fusion.24), kind=kOutput, calls=%fused_computation.23 | convolution fusion | flops 4432822272 | bytes 26804224 | tf_op jit(solution)/shard_map/dot_general | solution.py:126
  687.2 6.5 reduce-scatter.5.cloned.1.call-done
  693.7 1.9 fusion.18
  (57 shorter events, 1.8 us)
Async XLA Ops:
  6.5 5.2 copy-start.2
  6.5 6.1 copy-start.1
  6.5 75.9 %all-gather.6.cloned.1.call-start = ((), (), s32[]{:S(2)}) async-start(), calls=%async_computation.2 | async-start | bytes 3342336 | tf_op jit(solution)/shard_map/all_gather | solution.py:91
  8.0 5.3 copy-start.5
  11.7 140.0 %all-gather.8.cloned.1.call-start = ((), (), s32[]{:S(2)}) async-start(), calls=%async_computation.3 | async-start | bytes 3342336 | tf_op jit(solution)/shard_map/all_gather | solution.py:92
  12.5 191.2 %reduce-scatter.3.cloned.1.call-start = ((), (), s32[]{:S(2)}) async-start(), calls=%async_computation.4 | async-start | bytes 1179648 | tf_op jit(solution)/shard_map/reduce_scatter | solution.py:108
  156.5 3.8 copy-start
  166.5 3.8 copy-start
  176.6 3.8 copy-start
  186.6 3.8 copy-start
  192.5 11.3 %copy-start.3 = (bf16[192,2048]{1,0:T(8,128)(2,1)S(1)}, bf16[192,2048]{1,0:T(8,128)(2,1)}, u32[]{:S(2)}) copy-start(bf16[192,2048]{1,0:T(8,128)(2,1)} %param.13) | copy-start | bytes 2359300
  192.7 12.3 %copy-start.4 = (f32[2048]{0:T(1024)S(1)}, f32[2048]{0:T(1024)}, u32[]{:S(2)}) copy-start(f32[2048]{0:T(1024)} %param.20) | copy-start | bytes 24580
  196.9 152.0 %all-gather.10.cloned.1.call-start = ((), (), s32[]{:S(2)}) async-start(), calls=%async_computation.5 | async-start | bytes 12255232 | tf_op jit(solution)/shard_map/all_gather | solution.py:121
  197.5 293.7 %all-gather.12.cloned.1.call-start = ((), (), s32[]{:S(2)}) async-start(), calls=%async_computation.6 | async-start | bytes 12255232 | tf_op jit(solution)/shard_map/all_gather | solution.py:122
  198.1 475.9 %all-gather.14.cloned.1.call-start = ((), (), s32[]{:S(2)}) async-start(), calls=%async_computation.7 | async-start | bytes 12255232 | tf_op jit(solution)/shard_map/all_gather | solution.py:124
  198.6 495.1 %reduce-scatter.5.cloned.1.call-start = ((), (), s32[]{:S(2)}) async-start(), calls=%async_computation.8 | async-start | bytes 1179648 | tf_op jit(solution)/shard_map/reduce_scatter | solution.py:125
Sparse Core Ops, SparseCore 0:
  11.9 70.5 all-gather.5
  85.2 66.3 all-gather.7
  197.0 6.6 reduce-scatter.2
  206.4 142.5 all-gather.9
  351.5 139.5 all-gather.11
  493.7 180.2 all-gather.13
  687.3 6.3 reduce-scatter.4
where the time goes:
time: 703 us; the launch traced here: 702 us
  waiting for transfers between devices  609 us (87%)
  matrix products  41.2 us (6%)
  other arithmetic  23.7 us (3%)
  between operations  13.8 us (2%)
  local copies, waits for them, and re-layouts  11.4 us (2%)
    all_gather x1, waiting for transfers between devices, body(): down_whole = lax.all_gather(down_weight, 'sp', axis=1, tiled=True)  183 us
    all_gather x1, waiting for transfers between devices, body(): gate = add_rows(lax.all_gather(gate_weight, 'sp', axis=0, tiled=True))  141 us
    all_gather x1, waiting for transfers between devices, body(): up_part = add_rows(lax.all_gather(up_weight, 'sp', axis=0, tiled=True))  136 us
    all_gather x1, waiting for transfers between devices, body(): val_part = lax.all_gather(val_rows, 'sp', axis=0, tiled=True)  69.2 us
    all_gather x1, waiting for transfers between devices, body(): key_part = lax.all_gather(k_rot, 'sp', axis=0, tiled=True)  67.4 us
    reduce_sum x4, other arithmetic, key_block(): totals = totals * shrink + jnp.sum(weights, axis=-1)  14.2 us
  transfers between devices with their start and end apart: 7, of which 7 were waited for; matrix products, arithmetic and copies ran while one was open for 2% of the time, Pallas kernels for 0%

commit v1 on v0

--- a/solution.py
+++ b/solution.py
@@ -121,7 +121,8 @@
     gate = add_rows(lax.all_gather(gate_weight, "sp", axis=0, tiled=True))
     up_part = add_rows(lax.all_gather(up_weight, "sp", axis=0, tiled=True))
     hidden = (jax.nn.silu(gate) * up_part).astype(jnp.bfloat16)
-    down_whole = lax.all_gather(down_weight, "sp", axis=1, tiled=True)
+    earlier = lax.all_gather(down_weight, "sp")
+    down_whole = jnp.concatenate(earlier, axis=1)
     down = lax.psum_scatter(
         jnp.dot(hidden, down_whole, preferred_element_type=jnp.float32).astype(jnp.bfloat16),
         "tp",

time: 703 us -> 664 us (0.945)
  waiting for transfers between devices: 609 us -> 554 us
  local copies, waits for them, and re-layouts: 11.4 us -> 26.6 us
    all_gather x1, waiting for transfers between devices: 183 us -> 141 us  [body(): earlier = lax.all_gather(down_weight, 'sp')]
    reshape x0 -> x1, local copies, waits for them, and re-layouts: none -> 15.1 us  [body(): down_whole = jnp.concatenate(earlier, axis=1)]
    all_gather x1, waiting for transfers between devices: 141 us -> 127 us  [body(): gate = add_rows(lax.all_gather(gate_weight, 'sp', axis=0, tiled=True))]
  transfers between devices with their start and end apart: 7 -> 7, of which waited for: 7 -> 7; matrix products, arithmetic and copies ran while one was open for 2% -> 4% of each run, Pallas kernels for 0% -> 0%
where the time goes in v1:
time: 664 us; the launch traced here: 663 us
  waiting for transfers between devices  554 us (83%)
  matrix products  42.6 us (6%)
  local copies, waits for them, and re-layouts  26.6 us (4%)
  other arithmetic  23.7 us (4%)
  between operations  13.8 us (2%)
    all_gather x1, waiting for transfers between devices, body(): earlier = lax.all_gather(down_weight, 'sp')  141 us
    all_gather x1, waiting for transfers between devices, body(): up_part = add_rows(lax.all_gather(up_weight, 'sp', axis=0, tiled=True))  136 us
    all_gather x1, waiting for transfers between devices, body(): gate = add_rows(lax.all_gather(gate_weight, 'sp', axis=0, tiled=True))  127 us
    all_gather x1, waiting for transfers between devices, body(): val_part = lax.all_gather(val_rows, 'sp', axis=0, tiled=True)  69.2 us
    all_gather x1, waiting for transfers between devices, body(): key_part = lax.all_gather(k_rot, 'sp', axis=0, tiled=True)  67.4 us
    reshape x1, local copies, waits for them, and re-layouts, body(): down_whole = jnp.concatenate(earlier, axis=1)  15.1 us
    dot_general x1, matrix products, body(): jnp.dot(hidden, down_whole, preferred_element_type=jnp.float32)  14.6 us
    reduce_sum x4, other arithmetic, key_block(): totals = totals * shrink + jnp.sum(weights, axis=-1)  14.2 us
  transfers between devices with their start and end apart: 7, of which 7 were waited for; matrix products, arithmetic and copies ran while one was open for 4% of the time, Pallas kernels for 0%

profile of v1, /device:TPU:0, one launch (start us, length us, event | category | flops | bytes accessed | tf_op | source)
XLA Modules:
  0.0 663.3 jit_solution(6772892795275139343)
XLA Ops:
  6.6 1.1 reshape.201
  7.7 0.3 multiply_reduce_fusion.1
  8.0 0.9 multiply_multiply_fusion.1
  8.9 0.8 multiply_cosine_fusion.1
  9.7 0.7 subtract_convert_fusion.3
  10.4 1.3 pad_maximum_fusion.1
  11.8 0.7 reshape.197
  12.9 0.3 multiply_reduce_fusion
  13.4 0.3 multiply_multiply_fusion
  13.6 0.7 subtract_convert_fusion.1
  14.6 0.5 pad_maximum_fusion
  15.1 67.4 %all-gather.7.cloned.1.call-done = bf16[3072,4,128]{2,1,0:T(4,128)(2,1)} async-done(((bf16[192,4,128]{2,1,0:T(4,128)(2,1)}), bf16[3072,4,128]{2,1,0:T(4,128)(2,1)}) %all-gather.7.cloned.1.call-update) | async-done | bytes 3145744 | tf_op jit(solution)/shard_map/all_gather | solution.py:91
  82.5 69.2 %all-gather.9.cloned.1.call-done = bf16[3072,4,128]{2,1,0:T(4,128)(2,1)} async-done(((bf16[192,4,128]{2,1,0:T(4,128)(2,1)}), bf16[3072,4,128]{2,1,0:T(4,128)(2,1)}) %all-gather.9.cloned.1.call-update) | async-done | bytes 3145744 | tf_op jit(solution)/shard_map/all_gather | solution.py:92
  151.7 40.1 %while.15 = (s32[]{:T(128)}, f32[4,2,192]{2,1,0:T(2,128)S(1)}, f32[4,2,192]{2,1,0:T(2,128)S(1)}, f32[4,2,192,128]{3,2,1,0:T(8,128)S(1)}, bf16[4,768,4,128]{3,2,1...) while((s32[]{:T(128)}, f32[4,2,192]{2,1,0:T(2,128)S(1)}, ...), condition=%wide.region_5.6_spmd.clone, body=%wide.region_2.5_spmd.clone.sunk | while | flops 614014464 | bytes 39813256 | solution.py:99
  151.7 1.9 constant_dynamic-slice_fusion.3
  153.6 2.9 bitcast_reduce_fusion.2
  156.5 3.5 fusion.42
  160.3 1.4 fusion.44
  161.7 1.9 constant_dynamic-slice_fusion.3
  163.6 2.9 bitcast_reduce_fusion.2
  166.6 3.5 fusion.42
  170.3 1.4 fusion.44
  171.7 1.9 constant_dynamic-slice_fusion.3
  173.6 2.9 bitcast_reduce_fusion.2
  176.6 3.5 fusion.42
  180.3 1.4 fusion.44
  181.7 1.9 constant_dynamic-slice_fusion.3
  183.7 2.9 bitcast_reduce_fusion.2
  186.6 3.5 fusion.42
  190.3 1.4 fusion.44
  191.8 0.3 fusion.19
  192.0 0.4 copy.59
  192.5 0.3 convert_element_type.83
  192.8 4.1 convolution_convert_fusion.1
  196.9 0.5 all-gather.15.cloned.1.call-update
  197.5 0.5 all-gather.11.cloned.1.call-update
  198.1 0.5 all-gather.13.cloned.1.call-update
  198.7 5.1 reduce-scatter.3.cloned.1.call-done
  203.8 1.2 fusion.15
  205.2 2.5 all_gather.23
  207.7 141.2 %all-gather.15.cloned.1.call-done = bf16[45056,128]{1,0:T(8,128)(2,1)} async-done(((bf16[2816,128]{1,0:T(8,128)(2,1)}), bf16[45056,128]{1,0:T(8,128)(2,1)}) %all-gather.15.cloned.1.call-update) | async-done | bytes 11534352 | tf_op jit(solution)/shard_map/all_gather | solution.py:124
  348.9 15.1 %copy.60 = bf16[2816,16,128]{0,2,1:T(8,128)(2,1)} copy(bf16[2816,16,128]{2,0,1:T(8,128)(2,1)} %bitcast.62) | data formatting | bytes 23068672 | tf_op jit(solution)/shard_map/reshape | solution.py:125
  364.0 127.1 %all-gather.11.cloned.1.call-done = bf16[2048,2816]{1,0:T(8,128)(2,1)} async-done(((bf16[128,2816]{1,0:T(8,128)(2,1)}), bf16[2048,2816]{1,0:T(8,128)(2,1)}) %all-gather.11.cloned.1.call-update) | async-done | bytes 11534352 | tf_op jit(solution)/shard_map/all_gather | solution.py:121
  491.2 6.7 %fusion.24 = f32[192,2816]{1,0:T(8,128)S(1)} fusion(bf16[192,2048]{1,0:T(8,128)(2,1)S(1)} %all_gather.23, bf16[2048,2816]{1,0:T(8,128)(2,1)} %all-gather.11.cloned.1.call-done), kind=kOutput, calls=%fused_computation.69 | convolution fusion | flops 2214592512 | bytes 14483456 | tf_op jit(solution)/shard_map/dot_general | solution.py:119
  497.8 135.6 %all-gather.13.cloned.1.call-done = bf16[2048,2816]{1,0:T(8,128)(2,1)} async-done(((bf16[128,2816]{1,0:T(8,128)(2,1)}), bf16[2048,2816]{1,0:T(8,128)(2,1)}) %all-gather.13.cloned.1.call-update) | async-done | bytes 11534352 | tf_op jit(solution)/shard_map/all_gather | solution.py:122
  633.4 14.6 %convolution_convert_fusion = bf16[192,2048]{1,0:T(8,128)(2,1)} fusion(bf16[2816,2048]{0,1:T(8,128)(2,1)} %bitcast.63, bf16[192,2048]{1,0:T(8,128)(2,1)S(1)} %all_gather.23, bf16[2048,2816]{1,0:T(8,128)(2,1)} %all-gather.13.cloned.1.call-done, f32[192,2816]{1,0:T(8,128)S(1)} %fusion.24), kind=kOutput, calls=%fused_computation.23 | convolution fusion | flops 4432822272 | bytes 26804224 | tf_op jit(solution)/shard_map/dot_general | solution.py:127
  648.1 6.5 reduce-scatter.5.cloned.1.call-done
  654.6 1.9 fusion.18
  (58 shorter events, 2.0 us)
Async XLA Ops:
  6.5 5.2 copy-start.2
  6.5 6.1 copy-start.1
  6.5 75.9 %all-gather.7.cloned.1.call-start = ((), (), s32[]{:S(2)}) async-start(), calls=%async_computation.2 | async-start | bytes 3342336 | tf_op jit(solution)/shard_map/all_gather | solution.py:91
  8.0 5.3 copy-start.5
  11.7 140.0 %all-gather.9.cloned.1.call-start = ((), (), s32[]{:S(2)}) async-start(), calls=%async_computation.3 | async-start | bytes 3342336 | tf_op jit(solution)/shard_map/all_gather | solution.py:92
  12.5 191.2 %reduce-scatter.3.cloned.1.call-start = ((), (), s32[]{:S(2)}) async-start(), calls=%async_computation.4 | async-start | bytes 1179648 | tf_op jit(solution)/shard_map/reduce_scatter | solution.py:108
  156.5 3.8 copy-start
  166.5 3.8 copy-start
  176.6 3.8 copy-start
  186.6 3.8 copy-start
  192.5 11.3 %copy-start.3 = (bf16[192,2048]{1,0:T(8,128)(2,1)S(1)}, bf16[192,2048]{1,0:T(8,128)(2,1)}, u32[]{:S(2)}) copy-start(bf16[192,2048]{1,0:T(8,128)(2,1)} %param.13) | copy-start | bytes 2359300
  192.7 12.3 %copy-start.4 = (f32[2048]{0:T(1024)S(1)}, f32[2048]{0:T(1024)}, u32[]{:S(2)}) copy-start(f32[2048]{0:T(1024)} %param.20) | copy-start | bytes 24580
  196.9 152.0 %all-gather.15.cloned.1.call-start = ((), (), s32[]{:S(2)}) async-start(), calls=%async_computation.8 | async-start | bytes 12255232 | tf_op jit(solution)/shard_map/all_gather | solution.py:124
  197.5 293.7 %all-gather.11.cloned.1.call-start = ((), (), s32[]{:S(2)}) async-start(), calls=%async_computation.5 | async-start | bytes 12255232 | tf_op jit(solution)/shard_map/all_gather | solution.py:121
  198.1 435.4 %all-gather.13.cloned.1.call-start = ((), (), s32[]{:S(2)}) async-start(), calls=%async_computation.6 | async-start | bytes 12255232 | tf_op jit(solution)/shard_map/all_gather | solution.py:122
  198.6 455.9 %reduce-scatter.5.cloned.1.call-start = ((), (), s32[]{:S(2)}) async-start(), calls=%async_computation.7 | async-start | bytes 1179648 | tf_op jit(solution)/shard_map/reduce_scatter | solution.py:126
Sparse Core Ops, SparseCore 0:
  11.9 70.5 all-gather.6
  85.2 66.3 all-gather.8
  197.0 6.6 reduce-scatter.2
  206.4 142.5 all-gather.14
  351.5 139.5 all-gather.10
  493.8 139.5 all-gather.12
  648.2 6.3 reduce-scatter.4
